TPU v7x, 256 devices: a whole 4x4x8 slice. The times are simulated.
256 devices in a mesh: sp: 32 (over z, x), tp: 8 (over y, core).
Axes of the slice: x: 4, y: 4, z: 8, core: 2. Of those that a mesh axis runs over, the one named last changes fastest.
Arguments:
- resid: bfloat16 [8192, 4096], P('sp'), may hold values from -6 to 6
- queries: bfloat16 [8192, 3072], P('sp', 'tp'), may hold values from -1000 to 1000
- latent: bfloat16 [8192, 512], P('sp'), may hold values from -6 to 6
- rope_key: bfloat16 [8192, 64], P('sp'), may hold values from -6 to 6
- lat_gain: float32 [512], replicated, may hold values from 0.1 to 1.9
- kv_weight: bfloat16 [512, 4096], P(None, 'tp'), may hold values from -4 to 4
- out_gain: float32 [2048], P('tp'), may hold values from 0.1 to 1.9
- out_weight: bfloat16 [2048, 4096], P('tp'), may hold values from -0.125 to 0.125
- ffn_gain: float32 [4096], replicated, may hold values from 0.1 to 1.9
- gate_weight: bfloat16 [4096, 6144], P('sp', 'tp'), may hold values from -0.09375 to 0.09375
- up_weight: bfloat16 [4096, 6144], P('sp', 'tp'), may hold values from -0.09375 to 0.09375
- down_weight: bfloat16 [6144, 4096], P('tp', 'sp'), may hold values from -0.078125 to 0.078125
Outputs:
- result: bfloat16 [8192, 4096], P(('sp', 'tp'))
All inputs are finite; a program needn't handle non-finite values.
Results may differ from a plain program's by a relative error of at most 0.018.
Values may be sent and summed in bfloat16 or wider, within the bound.
A program may use at most 192 MiB of HBM per device.

v0:
```python
import math
import jax
import jax.numpy as jnp
from jax import lax
from jax.sharding import PartitionSpec as P

HEADS = 16
NOPE = 128
ROPE = 64
VDIM = 128
EPSILON = 1e-06
THETA = 10000.0
LOWEST = -1e30


def turned_gather(arrays, axis, dims):
    turned = [jnp.moveaxis(a, dim, 0) for a, dim in zip(arrays, dims)]
    both = jnp.concatenate([t.reshape(len(t), -1) for t in turned], axis=1)
    filled, at, outs = (lax.all_gather(both, axis, axis=0, tiled=True), 0, [])
    for t, dim in zip(turned, dims):
        slab = filled[:, at : at + t[0].size].reshape(-1, *t.shape[1:])
        outs.append(jnp.moveaxis(slab, 0, dim))
        at += t[0].size
    return tuple(outs)


def side_by_side(arrays, axis, dim, along):
    ends, at = ([], 0)
    for a in arrays[:-1]:
        at += a.shape[along]
        ends.append(at)
    both = jnp.concatenate(arrays, axis=along)
    return tuple(jnp.split(lax.all_gather(both, axis, axis=dim, tiled=True), ends, axis=along))


def sent_to_all(array, axis):
    copies = jnp.broadcast_to(array, (lax.axis_size(axis), *array.shape))
    return lax.all_to_all(copies, axis, split_axis=0, concat_axis=0, tiled=True)


def over_copies(array, axis):
    return sent_to_all(array, axis).sum(axis=0)


def cut_along(array, dim, devices):
    shape = array.shape
    parts = array.reshape(*shape[:dim], devices, shape[dim] // devices, *shape[dim + 1 :])
    return jnp.moveaxis(parts, dim, 0)


def summed_on_arrival(array, axis, dim):
    parts = cut_along(array, dim, lax.axis_size(axis))
    arrived = lax.all_to_all(parts, axis, split_axis=0, concat_axis=0, tiled=True)
    return arrived.astype(jnp.float32).sum(axis=0)


def laid_out(parts, dim):
    shape = list(parts.shape[1:])
    shape[dim] *= parts.shape[0]
    return jnp.moveaxis(parts, 0, dim).reshape(shape)


def gather_directly(array, axis, dim):
    parts = sent_to_all(array, axis)
    return laid_out(parts, dim)


def rotate(values, places):
    half = values.shape[-1] // 2
    inverse = THETA ** (-jnp.arange(half, dtype=jnp.float32) / half)
    angle = places[..., None] * inverse
    cosine = jnp.cos(angle)
    sine = jnp.sin(angle)
    first = values[..., :half]
    second = values[..., half:]
    return jnp.concatenate(
        [first * cosine - second * sine, first * sine + second * cosine], axis=-1
    )


def norm_rows(values, gain):
    wide = values.astype(jnp.float32)
    return wide * lax.rsqrt(jnp.mean(wide * wide, axis=-1, keepdims=True) + EPSILON) * gain


def make_keys(latent_piece, rotary_piece, start, lat_gain, kv_weight):
    normed = norm_rows(latent_piece, lat_gain).astype(jnp.bfloat16)
    key_value = jnp.dot(normed, kv_weight, preferred_element_type=jnp.float32).astype(jnp.bfloat16)
    key_index = start + jnp.arange(latent_piece.shape[0], dtype=jnp.int32)
    key_rope = rotate(rotary_piece.astype(jnp.float32), key_index.astype(jnp.float32)).astype(
        jnp.bfloat16
    )
    return (key_value, key_rope)


def body(
    resid,
    queries,
    latent,
    rope_key,
    lat_gain,
    kv_weight,
    out_gain,
    out_weight,
    ffn_gain,
    gate_weight,
    up_weight,
    down_weight,
):
    rows_here = resid.shape[0]
    first_row = lax.axis_index("sp") * rows_here
    heads_here = queries.shape[1] // (NOPE + ROPE)
    whole_gate, whole_up, whole_down = turned_gather(
        (gate_weight, up_weight, down_weight), "sp", (0, 0, 1)
    )
    query = queries.reshape(rows_here, heads_here, NOPE + ROPE)
    query_index = first_row + jnp.arange(rows_here, dtype=jnp.int32)
    query_nope = query[:, :, :NOPE]
    query_rope = rotate(
        query[:, :, NOPE:].astype(jnp.float32), query_index.astype(jnp.float32)[:, None]
    ).astype(jnp.bfloat16)
    scale = 1.0 / math.sqrt(NOPE + ROPE)

    def accumulate(state, key_value, key_rope):
        running_max, running_sum, weighted = state
        length = key_value.shape[0]
        key_value = key_value.reshape(length, heads_here, NOPE + VDIM)
        key_index = jnp.arange(length, dtype=jnp.int32)
        scores = jnp.einsum(
            "qhd,khd->hqk", query_nope, key_value[:, :, :NOPE], preferred_element_type=jnp.float32
        )
        scores = (
            scores
            + jnp.einsum("qhr,kr->hqk", query_rope, key_rope, preferred_element_type=jnp.float32)
        ) * scale
        allowed = (key_index[None, :] <= query_index[:, None])[None]
        scores = jnp.where(allowed, scores, LOWEST)
        new_max = jnp.maximum(running_max, jnp.max(scores, axis=-1))
        weights = jnp.where(allowed, jnp.exp(scores - new_max[:, :, None]), 0.0)
        running_sum = jnp.sum(weights, axis=-1)
        added = jnp.einsum(
            "hqk,khd->qhd",
            weights.astype(jnp.bfloat16),
            key_value[:, :, NOPE:],
            preferred_element_type=jnp.float32,
        )
        weighted = added
        return (new_max, running_sum, weighted)

    def unchanged(state):
        return state

    initial = (
        jnp.full((heads_here, rows_here), LOWEST, jnp.float32),
        jnp.zeros((heads_here, rows_here), jnp.float32),
        jnp.zeros((rows_here, heads_here, VDIM), jnp.float32),
    )
    own_value, own_rope = make_keys(latent, rope_key, first_row, lat_gain, kv_weight)
    pieces = side_by_side((own_value, own_rope), "sp", 0, 1)

    def update(state):
        return accumulate(state, pieces[0], pieces[1])

    running_max, running_sum, weighted = lax.cond(
        jnp.int32(0) < first_row + rows_here, update, unchanged, initial
    )
    attended = (weighted / jnp.transpose(running_sum)[:, :, None]).astype(jnp.bfloat16)
    attended_float = attended.reshape(rows_here, heads_here * VDIM).astype(jnp.float32)
    squares = over_copies(jnp.sum(attended_float * attended_float, axis=1), "tp")
    normed_out = attended_float * lax.rsqrt(squares / (HEADS * VDIM) + EPSILON)[:, None] * out_gain
    normed_out = normed_out.astype(jnp.bfloat16)
    share = rows_here // lax.axis_size("tp")
    own_first = lax.axis_index("tp") * share
    attn_sum = summed_on_arrival(
        jnp.dot(normed_out, out_weight, preferred_element_type=jnp.float32).astype(jnp.bfloat16),
        "tp",
        0,
    )
    own_resid = lax.dynamic_slice_in_dim(resid, own_first, share, 0)
    middle = (own_resid.astype(jnp.float32) + attn_sum).astype(jnp.bfloat16)
    normed_mid = gather_directly(norm_rows(middle, ffn_gain).astype(jnp.bfloat16), "tp", 0)
    gate = jnp.dot(normed_mid, whole_gate, preferred_element_type=jnp.float32)
    upward = jnp.dot(normed_mid, whole_up, preferred_element_type=jnp.float32)
    hidden = (jax.nn.silu(gate) * upward).astype(jnp.bfloat16)
    terms = jnp.dot(hidden, whole_down, preferred_element_type=jnp.float32)
    ffn_sum = summed_on_arrival(terms.astype(jnp.bfloat16), "tp", 0)
    return (middle.astype(jnp.float32) + ffn_sum).astype(jnp.bfloat16)


def solution(mesh):
    placed = (
        P("sp", None),
        P("sp", "tp"),
        P("sp", None),
        P("sp", None),
        P(),
        P(None, "tp"),
        P("tp"),
        P("tp", None),
        P(),
        P("sp", "tp"),
        P("sp", "tp"),
        P("tp", "sp"),
    )
    return jax.shard_map(
        body, mesh=mesh, in_specs=placed, out_specs=P(("sp", "tp"), None), check_vma=False
    )
```

profile of v0, /device:TPU:1, one launch (start us, length us, event | category | flops | bytes accessed | tf_op | source)
XLA Modules:
  0.0 339.7 jit_solution(4206966190794154403)
XLA Ops:
  6.5 0.0 copy-start
  6.5 0.0 all-gather.3.cloned.1.call-start
  6.6 0.9 convert_element_type.86
  7.5 0.2 multiply_cosine_fusion
  7.7 0.1 copy.62
  7.8 0.1 copy.63
  7.9 1.1 fusion.41
  9.0 1.5 convolution_convert_fusion.1
  10.5 0.8 pad_maximum_fusion.1
  11.4 0.0 all-gather.3.cloned.1.call-update
  11.4 0.0 all-gather.5.cloned.1.call-start
  11.4 1.1 copy.68
  12.5 1.1 copy.69
  13.6 1.8 pad_maximum_fusion
  15.4 0.0 all-gather.5.cloned.1.call-update
  15.4 1.1 copy.61
  16.6 106.4 %all-gather.3.cloned.1.call-done = bf16[8192,576]{1,0:T(8,128)(2,1)} async-done(((bf16[256,576]{1,0:T(8,128)(2,1)}), bf16[8192,576]{1,0:T(8,128)(2,1)}) %all-gather.3.cloned.1.call-update) | async-done | bytes 9437200 | tf_op jit(solution)/shard_map/all_gather | solution.py:33
  123.0 0.0 copy-start.3
  123.0 65.7 %conditional.1 = (f32[2,256]{1,0:T(2,128)S(1)}, f32[256,2,128]{0,2,1:T(8,128)S(1)}) conditional(s32[]{:T(128)} %convert_element_type.82, () %tuple.13, (s32[]{:T(128)}, s32[256]{0:T(256)S(1)}, bf16[256,2,192]{0,2,1:T(8,128)(2,1)S(1)}, bf16[8192,576]{1,0:T(8,128)(2,1)}, bf16[256,2,64]{0,2,1:T(8,128)(2,1)S(1)}) %tuple.36), branch_computations={%region_1.0_spmd, %region_2.5_spmd} | conditional | flops 2728394496 | bytes 147143728 | solution.py:164
  123.0 13.1 %copy.65 = bf16[8192,576]{0,1:T(8,128)(2,1)} copy(bf16[8192,576]{1,0:T(8,128)(2,1)} %get-tuple-element.53) | data formatting | bytes 18874368 | tf_op jit(solution)/shard_map
  136.1 7.9 %split.8 = bf16[8192,512]{0,1:T(8,128)(2,1)} slice(bf16[8192,576]{0,1:T(8,128)(2,1)} %copy.65), slice={[0:8192], [0:512]} | slice | bytes 16777216 | tf_op jit(solution)/shard_map/split | solution.py:33
  144.0 2.6 iota_compare_fusion
  146.6 9.4 %fusion.16 = f32[8192,256,2]{0,1,2:T(8,128)} fusion(bf16[256,2,64]{0,2,1:T(8,128)(2,1)S(1)} %get-tuple-element.25, bf16[8192,576]{0,1:T(8,128)(2,1)} %copy.65), kind=kOutput, calls=%fused_computation.15 | convolution fusion | flops 536870912 | bytes 17891328 | tf_op jit(solution)/shard_map/cond/branch_1_fun/qhr,kr->hqk/dot_general | solution.py:134
  156.0 0.1 copy.64
  156.2 0.0 copy-start.1
  156.2 15.2 %fusion.57 = (f32[2,256]{1,0:T(2,128)S(1)}, f32[2,256,8192]{2,1,0:T(8,128)}) fusion(f32[8192,256,2]{0,1,2:T(8,128)} %fusion.16, bf16[8192,2,256]{0,2,1:T(8,128)(2,1)} %bitcast.30, bf16[256,2,192]{2,0,1:T(8,128)(2,1)S(1)} %copy.64, pred[256,8192]{1,0:T(8,128)(4,1)} %iota_compare_fusion), kind=kOutput, calls=%fused_computation.76 | convolution fusion | flops 1090518528 | bytes 39979008 | tf_op jit(solution)/shard_map/cond/branch_1_fun/qhd,khd->hqk/dot_general | solution.py:129
  171.3 0.0 copy-done.1
  171.3 8.6 %fusion.11 = f32[256,2,128]{2,0,1:T(8,128)S(1)} fusion(bf16[8192,2,256]{0,2,1:T(8,128)(2,1)} %bitcast.31, f32[2,256,8192]{2,1,0:T(8,128)} %get-tuple-element.61, f32[2,256]{1,0:T(2,128)S(1)} %broadcast_maximum_fusion, pred[256,8192]{1,0:T(8,128)(4,1)S(1)} %copy-done.1), kind=kOutput, calls=%fused_computation.13 | convolution fusion | flops 1086324736 | bytes 23332864 | tf_op jit(solution)/shard_map/cond/branch_1_fun/hqk,khd->qhd/dot_general | solution.py:141
  180.0 0.1 copy.72
  180.1 8.5 %fusion.3 = f32[2,256]{1,0:T(2,128)S(1)} fusion(f32[2,256,8192]{2,1,0:T(8,128)} %get-tuple-element.61, f32[2,256]{1,0:T(2,128)S(1)} %broadcast_maximum_fusion, pred[256,8192]{1,0:T(8,128)(4,1)} %iota_compare_fusion), kind=kLoop, calls=%fused_computation.5 | loop fusion | flops 12582400 | bytes 18878464 | tf_op jit(solution)/shard_map/cond/branch_1_fun/reduce_sum | solution.py:140
  188.6 0.1 multiply_reduce_fusion
  188.7 10.3 %all_to_all.21 = f32[8,1,256]{2,1,0:T(1,128)S(1)} all-to-all(f32[8,1,256]{2,1,0:T(1,128)S(1)} %broadcast_in_dim.47), channel_id=1, replica_groups=mesh['sp'=32,'tp'=8] {'tp'}, dimensions={0} | all-to-all | bytes 16384 | tf_op jit(solution)/shard_map/all_to_all | solution.py:38
  199.1 0.0 copy-done.3
  199.1 0.0 copy-start.2
  199.1 0.1 fusion.51
  199.2 0.0 copy-done
  199.2 2.1 convolution_convert_fusion
  201.3 4.9 %all-to-all-start.1 = ((bf16[8,32,4096]{2,1,0:T(8,128)(2,1)}), bf16[8,32,4096]{2,1,0:T(8,128)(2,1)}, u32[]{:S(2)}, u32[]{:S(2)}) async-start(bf16[8,32,4096]{2,1,0:T(8,128)(2,1)} %bitcast.32), calls=%async_computation.1 | async-start | bytes 4194304 | tf_op jit(solution)/shard_map/all_to_all | solution.py:53
  206.1 26.3 %all-to-all-done.1 = bf16[8,32,4096]{2,1,0:T(8,128)(2,1)} async-done(((bf16[8,32,4096]{2,1,0:T(8,128)(2,1)}), bf16[8,32,4096]{2,1,0:T(8,128)(2,1)}, u32[]{:S(2)}, u32[]{:S(2)}) %all-to-all-start.1) | async-done | bytes 2097184 | tf_op jit(solution)/shard_map/all_to_all | solution.py:53
  232.5 2.0 convert_reduce_fusion.1
  234.5 1.2 fusion.44
  235.6 0.0 copy-done.2
  235.6 0.1 fusion.46
  235.8 0.2 broadcast_in_dim.48
  236.0 30.3 %all_to_all.22 = bf16[8,32,4096]{2,1,0:T(8,128)(2,1)} all-to-all(bf16[8,32,4096]{2,1,0:T(8,128)(2,1)S(1)} %broadcast_in_dim.48), channel_id=1, replica_groups=mesh['sp'=32,'tp'=8] {'tp'}, dimensions={0} | all-to-all | bytes 4194304 | tf_op jit(solution)/shard_map/all_to_all | solution.py:38
  266.3 14.7 %all-gather.5.cloned.1.call-done = bf16[4096,2304]{0,1:T(8,128)(2,1)} async-done(((bf16[128,2304]{0,1:T(8,128)(2,1)}), bf16[4096,2304]{0,1:T(8,128)(2,1)}) %all-gather.5.cloned.1.call-update) | async-done | bytes 18874384 | tf_op jit(solution)/shard_map/all_gather | solution.py:19
  281.0 5.2 %fusion.23 = f32[256,768]{1,0:T(8,128)S(1)} fusion(bf16[256,4096]{1,0:T(8,128)(2,1)} %bitcast.33, bf16[4096,2304]{0,1:T(8,128)(2,1)} %all-gather.5.cloned.1.call-done), kind=kOutput, calls=%fused_computation.24 | convolution fusion | flops 1610612736 | bytes 9175040 | tf_op jit(solution)/shard_map/dot_general | solution.py:182
  286.2 11.1 %fusion.25 = bf16[256,4096]{1,0:T(8,128)(2,1)} fusion(bf16[4096,2304]{0,1:T(8,128)(2,1)} %all-gather.5.cloned.1.call-done, bf16[256,4096]{1,0:T(8,128)(2,1)} %bitcast.34, f32[256,768]{1,0:T(8,128)S(1)} %fusion.23), kind=kOutput, calls=%fused_computation.27 | convolution fusion | flops 3223453696 | bytes 17563648 | tf_op jit(solution)/shard_map/dot_general | solution.py:185
  297.3 34.5 %all_to_all.23 = bf16[8,32,4096]{2,1,0:T(8,128)(2,1)S(1)} all-to-all(bf16[8,32,4096]{2,1,0:T(8,128)(2,1)} %bitcast.35), channel_id=1, replica_groups=mesh['sp'=32,'tp'=8] {'tp'}, dimensions={0} | all-to-all | bytes 4194304 | tf_op jit(solution)/shard_map/all_to_all | solution.py:53
  331.8 0.3 convert_reduce_fusion
  332.1 0.8 fusion.47
  (13 shorter events, 0.1 us)
Async XLA Ops:
  6.5 192.7 %copy-start = (bf16[256,4096]{1,0:T(8,128)(2,1)S(1)}, bf16[256,4096]{1,0:T(8,128)(2,1)}, u32[]{:S(2)}) copy-start(bf16[256,4096]{1,0:T(8,128)(2,1)} %param.21) | copy-start | bytes 6291460
  6.5 116.4 %all-gather.3.cloned.1.call-start = ((), (), s32[]{:S(2)}) async-start(), calls=%async_computation.4 | async-start | bytes 10813440 | tf_op jit(solution)/shard_map/all_gather | solution.py:33
  11.4 269.6 %all-gather.5.cloned.1.call-start = ((), (), s32[]{:S(2)}) async-start(), calls=%async_computation.5 | async-start | bytes 19464192 | tf_op jit(solution)/shard_map/all_gather | solution.py:19
  123.0 76.1 %copy-start.3 = (f32[256]{0:T(256)S(1)}, f32[256]{0:T(256)}, u32[]{:S(2)}) copy-start(f32[256]{0:T(256)} %param.20) | copy-start | bytes 3076
  156.2 15.2 %copy-start.1 = (pred[256,8192]{1,0:T(8,128)(4,1)S(1)}, pred[256,8192]{1,0:T(8,128)(4,1)}, u32[]{:S(2)}) copy-start(pred[256,8192]{1,0:T(8,128)(4,1)} %iota_compare_fusion) | copy-start | bytes 6291460 | tf_op jit(solution)/shard_map/cond
  199.1 36.5 %copy-start.2 = (f32[4096]{0:T(1024)S(1)}, f32[4096]{0:T(1024)}, u32[]{:S(2)}) copy-start(f32[4096]{0:T(1024)} %param.22) | copy-start | bytes 49156
  201.3 31.2 %all-to-all-start.1 = ((bf16[8,32,4096]{2,1,0:T(8,128)(2,1)}), bf16[8,32,4096]{2,1,0:T(8,128)(2,1)}, u32[]{:S(2)}, u32[]{:S(2)}) async-start(bf16[8,32,4096]{2,1,0:T(8,128)(2,1)} %bitcast.32), calls=%async_computation.1 | async-start | bytes 4194304 | tf_op jit(solution)/shard_map/all_to_all | solution.py:53
Sparse Core Ops, SparseCore 0:
  11.5 111.4 all-gather.2
  125.4 155.4 all-gather.4
where the time goes:
time: 341 us; the launch traced here: 340 us
  waiting for transfers between devices  147 us (43%)
  blocking collectives  75.1 us (22%)
  matrix products  53.1 us (16%)
  local copies, waits for them, and re-layouts  25 us (7%)
  other arithmetic  20.6 us (6%)
  between operations  13.5 us (4%)
  starting transfers between devices  4.9 us (1%)
    all_gather x1, waiting for transfers between devices, side_by_side(): lax.all_gather(both, axis, axis=dim, tiled=True)  106 us
    all_to_all x2, blocking collectives, sent_to_all(): return lax.all_to_all(copies, axis, split_axis=0, concat_axis=0, tiled=True)  40.6 us
    all_to_all x1, blocking collectives, summed_on_arrival(): lax.all_to_all(parts, axis, split_axis=0, concat_axis=0, tiled=True)  34.5 us
    all_to_all x1, waiting for transfers between devices, summed_on_arrival(): lax.all_to_all(parts, axis, split_axis=0, concat_axis=0, tiled=True)  26.3 us
    dot_general x1, matrix products, accumulate(): jnp.einsum('qhd,khd->hqk', query_nope, key_value[:, :, :NOPE], preferred_...  15.2 us
    all_gather x1, waiting for transfers between devices, turned_gather(): filled, at, outs = (lax.all_gather(both, axis, axis=0, tiled=True), 0, [])  14.7 us
    another operation x4, local copies, waits for them, and re-layouts  13.5 us
    dot_general x1, matrix products, body(): terms = jnp.dot(hidden, whole_down, preferred_element_type=jnp.float32)  11.1 us
  transfers between devices with their start and end apart: 3, of which 3 were waited for; matrix products, arithmetic and copies ran while one was open for 23% of the time, Pallas kernels for 0%

commit v1 on v0

--- a/solution.py
+++ b/solution.py
@@ -13,10 +13,15 @@
 LOWEST = -1e30
 
 
+def gather_over(x, axis, along):
+    stack = jnp.stack([x] * lax.axis_size(axis))
+    return jnp.concatenate(lax.all_to_all(stack, axis, 0, 0), axis=along)
+
+
 def turned_gather(arrays, axis, dims):
     turned = [jnp.moveaxis(a, dim, 0) for a, dim in zip(arrays, dims)]
     both = jnp.concatenate([t.reshape(len(t), -1) for t in turned], axis=1)
-    filled, at, outs = (lax.all_gather(both, axis, axis=0, tiled=True), 0, [])
+    filled, at, outs = (gather_over(both, axis, 0), 0, [])
     for t, dim in zip(turned, dims):
         slab = filled[:, at : at + t[0].size].reshape(-1, *t.shape[1:])
         outs.append(jnp.moveaxis(slab, 0, dim))

time: 341 us -> 743 us (2.18)
  blocking collectives: 75.1 us -> 456 us
  waiting for transfers between devices: 147 us -> 162 us
  local copies, waits for them, and re-layouts: 25 us -> 33.2 us
    all_to_all x0 -> x1, blocking collectives: none -> 413 us  [gather_over(): return jnp.concatenate(lax.all_to_all(stack, axis, 0, 0), axis=along)]
    all_to_all x2 -> x1, blocking collectives: 40.6 us -> 10.1 us  [sent_to_all(): return lax.all_to_all(copies, axis, split_axis=0, concat_axis=0, tiled=True)]
    all_to_all x0 -> x1, waiting for transfers between devices: none -> 25.7 us  [sent_to_all(): return lax.all_to_all(copies, axis, split_axis=0, concat_axis=0, tiled=True)]
    all_gather x1 -> x0, waiting for transfers between devices: 14.7 us -> none  [turned_gather(): filled, at, outs = (lax.all_gather(both, axis, axis=0, tiled=True), 0, [])]
    another operation x4 -> x5, local copies, waits for them, and re-layouts: 13.5 us -> 15.7 us
  transfers between devices with their start and end apart: 3 -> 3, of which waited for: 3 -> 3; matrix products, arithmetic and copies ran while one was open for 23% -> 0% of each run, Pallas kernels for 0% -> 0%
where the time goes in v1:
time: 743 us
  blocking collectives  456 us (61%)
  waiting for transfers between devices  162 us (22%)
  matrix products  51.1 us (7%)
  local copies, waits for them, and re-layouts  33.2 us (4%)
  other arithmetic  16.9 us (2%)
  between operations  13.6 us (2%)
  starting transfers between devices  9.41 us (1%)
    all_to_all x1, blocking collectives, gather_over(): return jnp.concatenate(lax.all_to_all(stack, axis, 0, 0), axis=along)  413 us
    all_gather x1, waiting for transfers between devices, side_by_side(): lax.all_gather(both, axis, axis=dim, tiled=True)  110 us
    all_to_all x1, blocking collectives, summed_on_arrival(): lax.all_to_all(parts, axis, split_axis=0, concat_axis=0, tiled=True)  32.6 us
    all_to_all x1, waiting for transfers between devices, summed_on_arrival(): lax.all_to_all(parts, axis, split_axis=0, concat_axis=0, tiled=True)  26.2 us
    all_to_all x1, waiting for transfers between devices, sent_to_all(): return lax.all_to_all(copies, axis, split_axis=0, concat_axis=0, tiled=True)  25.7 us
    dot_general x1, matrix products, accumulate(): jnp.einsum('qhd,khd->hqk', query_nope, key_value[:, :, :NOPE], preferred_...  14.9 us
  transfers between devices with their start and end apart: 3, of which 3 were waited for; matrix products, arithmetic and copies ran while one was open for 0% of the time, Pallas kernels for 0%

profile of v1, /device:TPU:1, one launch (start us, length us, event | category | flops | bytes accessed | tf_op | source)
XLA Modules:
  0.0 742.5 jit_solution(13898491181106861653)
XLA Ops:
  6.5 0.0 copy-start
  6.5 0.0 all-gather.2.cloned.1.call-start
  6.6 0.9 convert_element_type.86
  7.5 0.2 multiply_cosine_fusion
  7.7 0.1 copy.66
  7.8 0.1 copy.67
  7.9 1.1 fusion.41
  9.0 1.5 convolution_convert_fusion.1
  10.5 0.8 pad_maximum_fusion.1
  11.3 0.0 all-gather.2.cloned.1.call-update
  11.3 1.1 copy.65
  12.5 110.5 %all-gather.2.cloned.1.call-done = bf16[8192,576]{1,0:T(8,128)(2,1)} async-done(((bf16[256,576]{1,0:T(8,128)(2,1)}), bf16[8192,576]{1,0:T(8,128)(2,1)}) %all-gather.2.cloned.1.call-update) | async-done | bytes 9437200 | tf_op jit(solution)/shard_map/all_gather | solution.py:38
  122.9 0.0 copy-start.8
  122.9 64.9 %conditional.1 = (f32[2,256]{1,0:T(2,128)S(1)}, f32[256,2,128]{0,2,1:T(8,128)S(1)}) conditional(s32[]{:T(128)} %convert_element_type.82, () %tuple.13, (s32[]{:T(128)}, s32[256]{0:T(256)S(1)}, bf16[256,2,192]{0,2,1:T(8,128)(2,1)S(1)}, bf16[8192,576]{1,0:T(8,128)(2,1)}, bf16[256,2,64]{0,2,1:T(8,128)(2,1)S(1)}) %tuple.34), branch_computations={%region_1.0_spmd, %region_2.5_spmd} | conditional | flops 2728394496 | bytes 147143728 | solution.py:169
  122.9 13.1 %copy.69 = bf16[8192,576]{0,1:T(8,128)(2,1)} copy(bf16[8192,576]{1,0:T(8,128)(2,1)} %get-tuple-element.53) | data formatting | bytes 18874368 | tf_op jit(solution)/shard_map
  136.1 7.7 %split.8 = bf16[8192,512]{0,1:T(8,128)(2,1)} slice(bf16[8192,576]{0,1:T(8,128)(2,1)} %copy.69), slice={[0:8192], [0:512]} | slice | bytes 16777216 | tf_op jit(solution)/shard_map/split | solution.py:38
  143.8 2.7 iota_compare_fusion
  146.4 9.3 %fusion.16 = f32[8192,256,2]{0,1,2:T(8,128)} fusion(bf16[256,2,64]{0,2,1:T(8,128)(2,1)S(1)} %get-tuple-element.25, bf16[8192,576]{0,1:T(8,128)(2,1)} %copy.69), kind=kOutput, calls=%fused_computation.15 | convolution fusion | flops 536870912 | bytes 17891328 | tf_op jit(solution)/shard_map/cond/branch_1_fun/qhr,kr->hqk/dot_general | solution.py:139
  155.7 0.1 copy.68
  155.9 0.0 copy-start.2
  155.9 14.9 %fusion.57 = (f32[2,256]{1,0:T(2,128)S(1)}, f32[2,256,8192]{2,1,0:T(8,128)}) fusion(f32[8192,256,2]{0,1,2:T(8,128)} %fusion.16, bf16[8192,2,256]{0,2,1:T(8,128)(2,1)} %bitcast.33, bf16[256,2,192]{2,0,1:T(8,128)(2,1)S(1)} %copy.68, pred[256,8192]{1,0:T(8,128)(4,1)} %iota_compare_fusion), kind=kOutput, calls=%fused_computation.76 | convolution fusion | flops 1090518528 | bytes 39979008 | tf_op jit(solution)/shard_map/cond/branch_1_fun/qhd,khd->hqk/dot_general | solution.py:134
  170.8 0.0 copy-done.2
  170.8 8.6 %fusion.11 = f32[256,2,128]{2,0,1:T(8,128)S(1)} fusion(bf16[8192,2,256]{0,2,1:T(8,128)(2,1)} %bitcast.34, f32[2,256,8192]{2,1,0:T(8,128)} %get-tuple-element.61, f32[2,256]{1,0:T(2,128)S(1)} %broadcast_maximum_fusion, pred[256,8192]{1,0:T(8,128)(4,1)S(1)} %copy-done.2), kind=kOutput, calls=%fused_computation.13 | convolution fusion | flops 1086324736 | bytes 23332864 | tf_op jit(solution)/shard_map/cond/branch_1_fun/hqk,khd->qhd/dot_general | solution.py:146
  179.5 0.1 copy.77
  179.6 8.3 %fusion.3 = f32[2,256]{1,0:T(2,128)S(1)} fusion(f32[2,256,8192]{2,1,0:T(8,128)} %get-tuple-element.61, f32[2,256]{1,0:T(2,128)S(1)} %broadcast_maximum_fusion, pred[256,8192]{1,0:T(8,128)(4,1)} %iota_compare_fusion), kind=kLoop, calls=%fused_computation.5 | loop fusion | flops 12582400 | bytes 18878464 | tf_op jit(solution)/shard_map/cond/branch_1_fun/reduce_sum | solution.py:145
  187.9 0.1 multiply_reduce_fusion
  188.0 10.1 %all_to_all.26 = f32[8,1,256]{2,1,0:T(1,128)S(1)} all-to-all(f32[8,1,256]{2,1,0:T(1,128)S(1)} %broadcast_in_dim.47), channel_id=1, replica_groups=mesh['sp'=32,'tp'=8] {'tp'}, dimensions={0} | all-to-all | bytes 16384 | tf_op jit(solution)/shard_map/all_to_all | solution.py:43
  198.1 0.0 copy-done.8
  198.1 0.0 copy-start.7
  198.1 0.1 fusion.51
  198.2 0.0 copy-done
  198.2 2.1 convolution_convert_fusion
  200.3 4.2 all-to-all-start.1
  204.5 0.0 copy-start.5
  204.5 0.0 copy-start.6
  204.5 0.0 copy-start.4
  204.5 26.2 %all-to-all-done.1 = bf16[8,32,4096]{2,1,0:T(8,128)(2,1)S(1)} async-done(((bf16[8,32,4096]{2,1,0:T(8,128)(2,1)}), bf16[8,32,4096]{2,1,0:T(8,128)(2,1)S(1)}, u32[]{:S(2)}, u32[]{:S(2)}) %all-to-all-start.1) | async-done | bytes 2097184 | tf_op jit(solution)/shard_map/all_to_all | solution.py:58
  230.8 0.3 convert_reduce_fusion.1
  231.1 1.1 fusion.44
  232.2 0.0 copy-done.7
  232.2 0.1 fusion.46
  232.4 1.6 broadcast_in_dim.48
  233.9 5.2 all-to-all-start.2
  239.1 0.0 copy-done.5
  239.2 0.2 copy.72
  239.3 0.0 copy-done.6
  239.3 0.2 copy.73
  239.5 0.0 copy-done.4
  239.5 0.2 copy.74
  239.8 25.7 %all-to-all-done.2 = bf16[8,32,4096]{2,1,0:T(8,128)(2,1)} async-done(((bf16[8,32,4096]{2,1,0:T(8,128)(2,1)}), bf16[8,32,4096]{2,1,0:T(8,128)(2,1)}, u32[]{:S(2)}, u32[]{:S(2)}) %all-to-all-start.2) | async-done | bytes 2097184 | tf_op jit(solution)/shard_map/all_to_all | solution.py:43
  265.5 2.2 stack.2
  267.7 413.2 %all_to_all.27 = bf16[32,128,2304]{2,1,0:T(8,128)(2,1)S(1)} all-to-all(bf16[32,128,2304]{2,1,0:T(8,128)(2,1)S(1)} %stack.2), channel_id=1, replica_groups=mesh['sp'=32,'tp'=8] {'sp'}, dimensions={0} | all-to-all | bytes 37748736 | tf_op jit(solution)/shard_map/all_to_all | solution.py:18
  680.9 0.0 copy-start.3
  680.9 6.5 copy-done.3
  687.3 3.4 fusion.23
  690.7 0.0 copy-start.1
  690.8 11.2 %fusion.25 = bf16[256,4096]{1,0:T(8,128)(2,1)} fusion(bf16[4096,2304]{1,0:T(8,128)(2,1)} %bitcast.32, bf16[256,4096]{1,0:T(8,128)(2,1)} %bitcast.8, f32[256,768]{1,0:T(8,128)S(1)} %fusion.23), kind=kOutput, calls=%fused_computation.27 | convolution fusion | flops 3223453696 | bytes 17563648 | tf_op jit(solution)/shard_map/dot_general | solution.py:190
  702.0 32.6 %all_to_all.28 = bf16[8,32,4096]{2,1,0:T(8,128)(2,1)S(1)} all-to-all(bf16[8,32,4096]{2,1,0:T(8,128)(2,1)} %bitcast.36), channel_id=1, replica_groups=mesh['sp'=32,'tp'=8] {'tp'}, dimensions={0} | all-to-all | bytes 4194304 | tf_op jit(solution)/shard_map/all_to_all | solution.py:58
  734.6 0.3 convert_reduce_fusion
  734.9 0.8 fusion.47
  735.7 0.0 copy-done.1
  (14 shorter events, 0.2 us)
Async XLA Ops:
  6.5 191.7 %copy-start = (bf16[256,4096]{1,0:T(8,128)(2,1)S(1)}, bf16[256,4096]{1,0:T(8,128)(2,1)}, u32[]{:S(2)}) copy-start(bf16[256,4096]{1,0:T(8,128)(2,1)} %param.21) | copy-start | bytes 6291460
  6.5 116.4 %all-gather.2.cloned.1.call-start = ((), (), s32[]{:S(2)}) async-start(), calls=%async_computation.5 | async-start | bytes 10813440 | tf_op jit(solution)/shard_map/all_gather | solution.py:38
  122.9 75.2 %copy-start.8 = (f32[256]{0:T(256)S(1)}, f32[256]{0:T(256)}, u32[]{:S(2)}) copy-start(f32[256]{0:T(256)} %param.20) | copy-start | bytes 3076
  155.9 15.0 %copy-start.2 = (pred[256,8192]{1,0:T(8,128)(4,1)S(1)}, pred[256,8192]{1,0:T(8,128)(4,1)}, u32[]{:S(2)}) copy-start(pred[256,8192]{1,0:T(8,128)(4,1)} %iota_compare_fusion) | copy-start | bytes 6291460 | tf_op jit(solution)/shard_map/cond
  198.1 34.1 %copy-start.7 = (f32[4096]{0:T(1024)S(1)}, f32[4096]{0:T(1024)}, u32[]{:S(2)}) copy-start(f32[4096]{0:T(1024)} %param.22) | copy-start | bytes 49156
  200.3 30.4 %all-to-all-start.1 = ((bf16[8,32,4096]{2,1,0:T(8,128)(2,1)}), bf16[8,32,4096]{2,1,0:T(8,128)(2,1)S(1)}, u32[]{:S(2)}, u32[]{:S(2)}) async-start(bf16[8,32,4096]{2,1,0:T(8,128)(2,1)} %bitcast.35), calls=%async_computation.1 | async-start | bytes 4194304 | tf_op jit(solution)/shard_map/all_to_all | solution.py:58
  204.5 34.6 %copy-start.5 = (bf16[128,768]{1,0:T(8,128)(2,1)S(1)}, bf16[128,768]{1,0:T(8,128)(2,1)}, u32[]{:S(2)}) copy-start(bf16[128,768]{1,0:T(8,128)(2,1)} %param.23) | copy-start | bytes 589828
  204.5 34.8 %copy-start.6 = (bf16[128,768]{1,0:T(8,128)(2,1)S(1)}, bf16[128,768]{1,0:T(8,128)(2,1)}, u32[]{:S(2)}) copy-start(bf16[128,768]{1,0:T(8,128)(2,1)} %param.24) | copy-start | bytes 589828
  204.5 35.0 %copy-start.4 = (bf16[768,128]{1,0:T(8,128)(2,1)S(1)}, bf16[768,128]{1,0:T(8,128)(2,1)}, u32[]{:S(2)}) copy-start(bf16[768,128]{1,0:T(8,128)(2,1)} %param.25) | copy-start | bytes 589828
  233.9 31.5 %all-to-all-start.2 = ((bf16[8,32,4096]{2,1,0:T(8,128)(2,1)}), bf16[8,32,4096]{2,1,0:T(8,128)(2,1)}, u32[]{:S(2)}, u32[]{:S(2)}) async-start(bf16[8,32,4096]{2,1,0:T(8,128)(2,1)} %broadcast_in_dim.48), calls=%async_computation.2 | async-start | bytes 4194304 | tf_op jit(solution)/shard_map/all_to_all | solution.py:43
  680.9 6.5 copy-start.3
  690.7 44.9 %copy-start.1 = (bf16[256,4096]{1,0:T(8,128)(2,1)S(1)}, bf16[256,4096]{1,0:T(8,128)(2,1)}, u32[]{:S(2)}) copy-start(bf16[256,4096]{1,0:T(8,128)(2,1)} %param.21) | copy-start | bytes 6291460
Sparse Core Ops, SparseCore 0:
  11.5 111.4 all-gather.1
